TPU v7x, 128 devices: a whole 4x4x4 slice. The times are simulated.
128 devices in a mesh: sp: 32 (over z, y, core), tp: 4 (over x).
Axes of the slice: x: 4, y: 4, z: 4, core: 2. Of those that a mesh axis runs over, the one named last changes fastest.
Arguments:
- residual: bfloat16 [32768, 2048], P('sp'), may hold values from -6 to 6
- small_heads: bfloat16 [32768, 1024], P('sp', 'tp'), may hold values from -6 to 6
- large_heads: bfloat16 [32768, 1024], P('sp', 'tp'), may hold values from -6 to 6
- state_keys: bfloat16 [32768, 8, 128], P('sp', 'tp'), may hold values from -6 to 6
- state_queries: bfloat16 [32768, 8, 128], P('sp', 'tp'), may hold values from -6 to 6
- small_gate: bfloat16 [32768, 1024], P('sp', 'tp'), may hold values from -6 to 6
- large_gate: bfloat16 [32768, 1024], P('sp', 'tp'), may hold values from -6 to 6
- small_step: float32 [32768, 16], P('sp', 'tp'), may hold values from -3 to 2
- large_step: float32 [32768, 8], P('sp', 'tp'), may hold values from -3 to 2
- small_taps: bfloat16 [4, 1024], P(None, 'tp'), may hold values from -3 to 3
- large_taps: bfloat16 [4, 1024], P(None, 'tp'), may hold values from -3 to 3
- key_taps: bfloat16 [4, 8, 128], P(None, 'tp'), may hold values from -3 to 3
- query_taps: bfloat16 [4, 8, 128], P(None, 'tp'), may hold values from -3 to 3
- small_decay: float32 [16], P('tp'), may hold values from -12 to -2, as said below
- large_decay: float32 [8], P('tp'), may hold values from -12 to -2, as said below
- small_gain: bfloat16 [1024], P('tp'), may hold values from 0.099609375 to 1.8984375
- large_gain: bfloat16 [1024], P('tp'), may hold values from 0.099609375 to 1.8984375
- small_out: bfloat16 [1024, 2048], P('tp'), may hold values from -0.125 to 0.125
- large_out: bfloat16 [1024, 2048], P('tp'), may hold values from -0.125 to 0.125
- mixer_gain: bfloat16 [2048], replicated, may hold values from 0.099609375 to 1.8984375
- ffn_in_gain: bfloat16 [2048], replicated, may hold values from 0.099609375 to 1.8984375
- gate_proj: bfloat16 [2048, 5632], P('sp', 'tp'), may hold values from -0.125 to 0.125
- up_proj: bfloat16 [2048, 5632], P('sp', 'tp'), may hold values from -0.125 to 0.125
- down_proj: bfloat16 [2048, 5632], P('sp', 'tp'), may hold values from -0.078125 to 0.078125
- ffn_out_gain: bfloat16 [2048], replicated, may hold values from 0.099609375 to 1.8984375
Outputs:
- updated: bfloat16 [32768, 2048], P(('sp', 'tp'))
Inputs may be any that keep to these rules, and one draw needn't show every extreme that they name: `small_decay`: log decay rates of the first group. `large_decay`: log decay rates of the second group.
All inputs are finite; a program needn't handle non-finite values.
Results may differ from a plain program's by a relative error of at most 0.014.
Values may be sent and summed in bfloat16 or wider, within the bound.
No kernel may reach another device: no remote copies, remote signals or barrier semaphores. Data moves between devices by JAX's collectives and lax.ppermute only.
A program may use at most 192 MiB of HBM per device.

v0:
```python
import jax
import jax.numpy as jnp
from jax import lax
from jax.sharding import Mesh
from jax.sharding import PartitionSpec as P

BLOCK = 128
SP = ("sp_0", "sp_1", "sp_2")
SP_TP = ("sp_0", "sp_1", "sp_2", "tp")
EPS = 1e-06


def passed_along(block, axis, distance):
    devices = range(lax.axis_size(axis))
    route = [(i - distance, i) for i in devices if i - distance in devices]
    return lax.ppermute(block, axis, route)


def nothing_yet(array, identity):
    return jax.tree.map(
        lambda a, e: jnp.broadcast_to(jnp.asarray(e, a.dtype), a.shape), array, identity
    )


def collected_together(array, axis):
    leaves = jax.tree.leaves(array)
    sequence = sorted(range(len(leaves)), key=lambda k: -leaves[k].size)
    width = (1, *leaves[sequence[0]].shape)[-1]
    lines = [
        jnp.pad(leaves[k].reshape(-1), (0, -leaves[k].size % width)).reshape(-1, width)
        for k in sequence
    ]
    both, at, found = (lax.all_gather(jnp.concatenate(lines), axis), 0, {})
    for k, line in zip(sequence, lines):
        slab = both[:, at : at + len(line)].reshape(len(both), -1)
        found[k] = slab[:, : leaves[k].size].reshape(-1, *leaves[k].shape)
        at += len(line)
    numbers = iter(range(len(leaves)))
    return jax.tree.map(lambda _: found[next(numbers)], array)


def prefix_by_axis(array, axes, combine, identity):
    before = start = nothing_yet(array, identity)
    subtotal = array
    for axis in reversed(axes):
        peers, position = (lax.axis_size(axis), lax.axis_index(axis))
        pieces = collected_together(
            jax.tree.map(
                lambda part, kind: part.astype(kind),
                subtotal,
                (jnp.bfloat16, jnp.bfloat16, jnp.bfloat16, jnp.bfloat16),
            ),
            axis,
        )
        inside, subtotal = (start, start)
        for k in range(peers):
            passed = k < position
            subtotal = combine(
                subtotal, jax.tree.map(lambda part, own: part[k].astype(own.dtype), pieces, array)
            )
            inside = jax.tree.map(lambda new, old: jnp.where(passed, new, old), subtotal, inside)
        before = combine(inside, before)
    return before


def in_one_piece(arrays, axis, dim, along):
    both = jnp.concatenate(arrays, axis=along)
    whole, at, finished = (lax.all_gather(both, axis, axis=dim, tiled=True), 0, [])
    for a in arrays:
        finished.append(lax.slice_in_dim(whole, at, at + a.shape[along], axis=along))
        at += a.shape[along]
    return tuple(finished)


def in_order(pieces, dim):
    pieces = jnp.moveaxis(pieces, 0, dim)
    dims = pieces.shape
    return pieces.reshape(*dims[:dim], dims[dim] * dims[dim + 1], *dims[dim + 2 :])


def all_blocks(array, axes, sequence):
    pieces = array
    for k in sequence:
        pieces = lax.all_gather(pieces, axes[k])
    done = sequence[::-1]
    back = [done.index(k) for k in range(len(axes))]
    pieces = pieces.transpose(*back, *range(len(axes), pieces.ndim))
    return pieces.reshape(-1, *array.shape)


def gather_axes(array, axes, sequence, dim):
    return in_order(all_blocks(array, axes, sequence), dim)


def causal_taps(extended, tap_weights, length):
    kernel_len = tap_weights.shape[0]
    summed = jnp.zeros((length,) + extended.shape[1:], jnp.float32)
    for offset in range(kernel_len):
        window_rows = extended[offset : offset + length].astype(jnp.float32)
        summed = summed + tap_weights[offset].astype(jnp.float32) * window_rows
    return jax.nn.silu(summed).astype(jnp.bfloat16)


def block_pass(values, key_rows, queries, step_sizes, decay_rates):
    length, groups, head_count, head_dim = values.shape
    block_count = length // BLOCK
    state_len = key_rows.shape[-1]
    log_decay = -step_sizes * decay_rates
    causal = jnp.tril(jnp.ones((BLOCK, BLOCK), dtype=bool))

    def one_block(carry_state, block):
        block_values, block_keys, block_queries, block_steps, block_decay = block
        cumulative = jnp.cumsum(block_decay, axis=0)
        scores = jnp.einsum(
            "lgn,sgn->gls", block_queries, block_keys, preferred_element_type=jnp.float32
        )
        cum_heads = jnp.transpose(cumulative, (1, 2, 0))
        gap_matrix = cum_heads[:, :, :, None] - cum_heads[:, :, None, :]
        decays = jnp.exp(jnp.where(causal, gap_matrix, -jnp.inf))
        step_heads = jnp.transpose(block_steps, (1, 2, 0))[:, :, None, :]
        weights = (scores[:, None] * decays * step_heads).astype(jnp.bfloat16)
        inside = jnp.einsum(
            "ghls,sghp->lghp", weights, block_values, preferred_element_type=jnp.float32
        )
        carried = jnp.einsum("lgn,ghpn->lghp", block_queries.astype(jnp.float32), carry_state)
        carried = carried * jnp.exp(cumulative)[..., None]
        tail_sum = cumulative[-1]
        scaled = (
            block_values.astype(jnp.float32)
            * (block_steps * jnp.exp(tail_sum - cumulative))[..., None]
        )
        fresh_state = jnp.einsum(
            "lghp,lgn->ghpn",
            scaled.astype(jnp.bfloat16),
            block_keys,
            preferred_element_type=jnp.float32,
        )
        next_state = carry_state * jnp.exp(tail_sum)[..., None, None] + fresh_state
        return (next_state, (inside + carried, cumulative))

    blocked = (
        values.reshape(block_count, BLOCK, groups, head_count, head_dim),
        key_rows.reshape(block_count, BLOCK, groups, state_len),
        queries.reshape(block_count, BLOCK, groups, state_len),
        step_sizes.reshape(block_count, BLOCK, groups, head_count),
        log_decay.reshape(block_count, BLOCK, groups, head_count),
    )
    start_state = jnp.zeros((groups, head_count, head_dim, state_len), jnp.float32)
    end_state, (outputs, cumulative) = lax.scan(one_block, start_state, blocked)
    tail_sums = cumulative[:, -1]
    offsets = jnp.cumsum(tail_sums, axis=0) - tail_sums
    device_cum = (cumulative + offsets[:, None]).reshape(length, groups, head_count)
    return (
        outputs.reshape(length, groups, head_count, head_dim),
        device_cum,
        end_state,
        jnp.sum(tail_sums, axis=0),
    )


def head_group(values, key_rows, queries, step_raw, decay_log):
    length = values.shape[0]
    head_count = step_raw.shape[1]
    groups = key_rows.shape[1]
    per_group = head_count // groups
    head_dim = values.shape[1] // head_count
    step_sizes = jax.nn.softplus(step_raw).reshape(length, groups, per_group)
    decay_rates = jnp.exp(decay_log).reshape(groups, per_group)
    return block_pass(
        values.reshape(length, groups, per_group, head_dim),
        key_rows,
        queries,
        step_sizes,
        decay_rates,
    )


def add_entering(outputs, queries, device_cum, entering):
    extra = jnp.einsum("lgn,ghpn->lghp", queries.astype(jnp.float32), entering)
    return outputs + extra * jnp.exp(device_cum)[..., None]


def unit_rms(values):
    return values * lax.rsqrt(jnp.mean(values * values, axis=-1, keepdims=True) + EPS)


def gate_and_norm(mixed_heads, gate_raw, gain):
    length, groups, per_group, head_dim = mixed_heads.shape
    gated = mixed_heads.reshape(length, -1) * jax.nn.silu(gate_raw.astype(jnp.float32))
    normed = unit_rms(gated.reshape(length, groups * per_group, head_dim))
    return (normed.reshape(length, -1) * gain.astype(jnp.float32)).astype(jnp.bfloat16)


def local(
    residual,
    small_heads,
    large_heads,
    state_keys,
    state_queries,
    small_gate,
    large_gate,
    small_step,
    large_step,
    small_taps,
    large_taps,
    key_taps,
    query_taps,
    small_decay,
    large_decay,
    small_gain,
    large_gain,
    small_out,
    large_out,
    mixer_gain,
    ffn_in_gain,
    gate_proj,
    up_proj,
    down_proj,
    ffn_out_gain,
):
    length = residual.shape[0]
    halo_rows = small_taps.shape[0] - 1
    first_row = length - halo_rows
    previous = passed_along(
        (
            small_heads[first_row:],
            large_heads[first_row:],
            state_keys[first_row:],
            state_queries[first_row:],
        ),
        SP,
        1,
    )
    small_conv = causal_taps(
        jnp.concatenate([previous[0], small_heads], axis=0), small_taps, length
    )
    large_conv = causal_taps(
        jnp.concatenate([previous[1], large_heads], axis=0), large_taps, length
    )
    key_conv = causal_taps(jnp.concatenate([previous[2], state_keys], axis=0), key_taps, length)
    query_conv = causal_taps(
        jnp.concatenate([previous[3], state_queries], axis=0), query_taps, length
    )
    small_out_local, small_cum, small_end, small_total = head_group(
        small_conv, key_conv[:, 0:1], query_conv[:, 0:1], small_step, small_decay
    )
    large_out_local, large_cum, large_end, large_total = head_group(
        large_conv, key_conv[:, 1:2], query_conv[:, 1:2], large_step, large_decay
    )

    def join(earlier, later):
        return (
            earlier[0] * jnp.exp(later[1])[..., None, None] + later[0],
            earlier[1] + later[1],
            earlier[2] * jnp.exp(later[3])[..., None, None] + later[2],
            earlier[3] + later[3],
        )

    identity_parts = (
        jnp.zeros_like(small_end),
        jnp.zeros_like(small_total),
        jnp.zeros_like(large_end),
        jnp.zeros_like(large_total),
    )
    entered = prefix_by_axis(
        (small_end, small_total, large_end, large_total), SP, join, identity_parts
    )
    small_enter = entered[0]
    large_enter = entered[2]
    small_mix = add_entering(small_out_local, query_conv[:, 0:1], small_cum, small_enter)
    large_mix = add_entering(large_out_local, query_conv[:, 1:2], large_cum, large_enter)
    small_normed = gate_and_norm(small_mix, small_gate, small_gain)
    large_normed = gate_and_norm(large_mix, large_gate, large_gain)
    partial_value = jnp.dot(small_normed, small_out, preferred_element_type=jnp.float32)
    partial_value = partial_value + jnp.dot(
        large_normed, large_out, preferred_element_type=jnp.float32
    )
    mix = lax.psum(partial_value.astype(jnp.bfloat16), "tp").astype(jnp.float32)
    mixed = residual.astype(jnp.float32) + unit_rms(mix) * mixer_gain.astype(jnp.float32)
    normed_in = (unit_rms(mixed) * ffn_in_gain.astype(jnp.float32)).astype(jnp.bfloat16)
    pieces = in_one_piece((gate_proj, up_proj), SP, 0, 1)
    gate = jnp.dot(normed_in, pieces[0], preferred_element_type=jnp.float32)
    up_values = jnp.dot(normed_in, pieces[1], preferred_element_type=jnp.float32)
    down_full = gather_axes(down_proj, (("sp_0", "sp_1"), "sp_2"), (0, 1), 0)
    hidden = (jax.nn.silu(gate) * up_values).astype(jnp.bfloat16)
    share = length // lax.axis_size("tp")
    ffn = lax.psum_scatter(
        lax.dot_general(
            hidden, down_full, (((1,), (1,)), ((), ())), preferred_element_type=jnp.float32
        ).astype(jnp.bfloat16),
        "tp",
        scatter_dimension=0,
        tiled=True,
    ).astype(jnp.float32)
    own_rows = lax.dynamic_slice_in_dim(mixed, lax.axis_index("tp") * share, share, 0)
    updated = own_rows + 0.5 * unit_rms(ffn) * ffn_out_gain.astype(jnp.float32)
    return updated.astype(jnp.bfloat16)


def solution(mesh):
    torus = Mesh(mesh.devices.reshape(4, 4, 2, mesh.shape["tp"]), ("sp_0", "sp_1", "sp_2", "tp"))
    in_specs = (
        P(SP, None),
        P(SP, "tp"),
        P(SP, "tp"),
        P(SP, "tp", None),
        P(SP, "tp", None),
        P(SP, "tp"),
        P(SP, "tp"),
        P(SP, "tp"),
        P(SP, "tp"),
        P(None, "tp"),
        P(None, "tp"),
        P(None, "tp", None),
        P(None, "tp", None),
        P("tp"),
        P("tp"),
        P("tp"),
        P("tp"),
        P("tp", None),
        P("tp", None),
        P(),
        P(),
        P(SP, "tp"),
        P(SP, "tp"),
        P(SP, "tp"),
        P(),
    )
    out_specs = P(SP_TP, None)
    return jax.shard_map(local, mesh=torus, in_specs=in_specs, out_specs=out_specs, check_vma=False)
```

profile of v0, /device:TPU:1, one launch (start us, length us, event | category | flops | bytes accessed | tf_op | source)
XLA Modules:
  0.0 482.5 jit_solution(811788357132697715)
XLA Ops:
  9.0 4.6 collective-permute-start
  13.6 1.1 copy.228
  14.7 1.9 collective-permute-start.1
  16.6 1.1 copy.231
  18.5 3.6 collective-permute-start.2
  23.0 1.9 collective-permute-start.3
  24.9 2.0 copy.226
  27.0 2.1 copy.240
  35.7 1.2 copy.248
  39.0 1.2 copy.253
  41.0 3.1 fusion.118
  45.9 2.5 multiply_convert_fusion.9
  49.2 83.8 %while.30 = (s32[]{:T(128)}, f32[1,4,64,128]{3,2,1,0:T(8,128)S(1)}, f32[8,128,1,4,64]{1,0,4,3,2:T(8,128)}, f32[8,128,1,4]{3,1,2,0:T(8,128)}, f32[8,128,1,4]{3,1,...) while((s32[]{:T(128)}, f32[1,4,64,128]{3,2,1,0:T(8,128)S(1)}, ...), condition=%wide.region_2.3_spmd.clone, body=%wide.region_0.2_spmd.clone.sunk | while | flops 30065156 | bytes 1596155 | solution.py:149
  53.5 1.1 fusion.250
  54.6 4.4 dynamic_update_slice.27
  64.0 1.1 fusion.250
  65.1 4.4 dynamic_update_slice.27
  74.4 1.1 fusion.250
  75.6 4.4 dynamic_update_slice.27
  84.9 1.1 fusion.250
  86.0 4.4 dynamic_update_slice.27
  95.4 1.1 fusion.250
  96.5 4.4 dynamic_update_slice.27
  105.9 1.1 fusion.250
  107.0 4.4 dynamic_update_slice.27
  116.3 1.1 fusion.250
  117.5 4.4 dynamic_update_slice.27
  126.8 1.1 fusion.250
  127.9 4.4 dynamic_update_slice.27
  134.7 3.0 fusion.119
  138.7 86.1 %while.31 = (s32[]{:T(128)}, f32[1,2,128,128]{3,2,1,0:T(8,128)S(1)}, f32[8,128,1,2,128]{1,0,4,3,2:T(8,128)}, f32[8,128,1,2]{3,1,2,0:T(8,128)}, f32[8,128,1,2]{3,...) while((s32[]{:T(128)}, ...), condition=%wide.region_5.6_spmd.clone, body=%wide.region_3.5_spmd.clone.sunk | while | flops 29868292 | bytes 1569483 | solution.py:149
  143.0 1.1 fusion.266
  144.1 4.8 dynamic_update_slice.29
  153.8 1.1 fusion.266
  154.9 4.8 dynamic_update_slice.29
  165.7 4.8 dynamic_update_slice.29
  176.4 4.8 dynamic_update_slice.29
  187.2 4.8 dynamic_update_slice.29
  198.0 4.8 dynamic_update_slice.29
  208.7 4.8 dynamic_update_slice.29
  219.5 4.8 dynamic_update_slice.29
  225.7 2.1 all-gather.5
  228.6 11.5 %all-gather.6 = bf16[4,514,128]{2,1,0:T(8,128)(2,1)S(1)} all-gather(bf16[1,514,128]{2,1,0:T(8,128)(2,1)S(1)} %maximum_bitcast_fusion.1), channel_id=3, replica_groups=mesh['sp_0'=4,'sp_1'=4,'sp_2'=2,'tp'=4] {'sp_1'}, dimensions={0}, use_global_device_ids=true | all-gather | bytes 657920 | tf_op jit(solution)/shard_map/all_gather | solution.py:33
  241.5 10.9 %all-gather.7 = bf16[4,514,128]{2,1,0:T(8,128)(2,1)S(1)} all-gather(bf16[1,514,128]{2,1,0:T(8,128)(2,1)S(1)} %maximum_bitcast_fusion.2), channel_id=4, replica_groups=mesh['sp_0'=4,'sp_1'=4,'sp_2'=2,'tp'=4] {'sp_0'}, dimensions={0}, use_global_device_ids=true | all-gather | bytes 657920 | tf_op jit(solution)/shard_map/all_gather | solution.py:33
  253.3 1.9 add_exponential_fusion.1
  255.2 2.4 reshape.954
  258.5 1.2 copy.247
  259.8 2.4 reshape.977
  263.0 1.9 add_exponential_fusion
  264.9 1.2 copy.252
  266.2 1.5 fusion.141
  267.7 1.5 fusion.95
  270.5 1.4 fusion.135
  273.0 1.3 fusion.191
  274.4 3.3 add_convert_fusion
  279.7 94.6 %all-reduce.8.cloned.1.call-done = bf16[1024,2048]{1,0:T(8,128)(2,1)} async-done(((bf16[1024,2048]{1,0:T(8,128)(2,1)}), bf16[1024,2048]{1,0:T(8,128)(2,1)}) %all-reduce.8.cloned.1.call-update) | async-done | bytes 4194320 | tf_op jit(solution)/shard_map/psum | solution.py:278
  374.3 3.2 fusion.74
  377.8 6.0 %multiply_reduce_fusion = (f32[1024]{0:T(1024)S(1)}, f32[1024,2048]{1,0:T(8,128)}) fusion(f32[2048]{0:T(1024)S(1)} %convert_element_type.718, f32[1024]{0:T(1024)S(1)} %add_rsqrt_fusion.3, bf16[1024,2048]{1,0:T(8,128)(2,1)S(1)} %copy-done.2, bf16[1024,2048]{1,0:T(8,128)(2,1)} %param.29), kind=kLoop, calls=%fused_computation.98 | loop fusion | flops 14679040 | bytes 16793600 | tf_op jit(solution)/shard_map/reduce_sum | solution.py:184
  383.8 5.8 %copy.254 = bf16[16,2,64,1408]{3,2,1,0:T(8,128)(2,1)} copy(bf16[16,2,64,1408]{3,2,0,1:T(8,128)(2,1)} %bitcast.557) | data formatting | bytes 11534336 | tf_op jit(solution)/shard_map/transpose | solution.py:87
  389.6 12.6 %fusion.79 = f32[1024,1408]{1,0:T(8,128)} fusion(bf16[2048,2816]{1,0:T(8,128)(2,1)} %all-gather.12.cloned.1.call-done, f32[1024,2048]{1,0:T(8,128)} %get-tuple-element.310, f32[2048]{0:T(1024)S(1)} %convert_element_type.719, f32[1024]{0:T(1024)S(1)} %add_rsqrt_fusion.2), kind=kOutput, calls=%fused_computation.102 | convolution fusion | flops 5911871488 | bytes 19935232 | tf_op jit(solution)/shard_map/dot_general | solution.py:282
  402.2 21.5 %fusion.86 = bf16[1024,2048]{1,0:T(8,128)(2,1)} fusion(bf16[2048,1408]{1,0:T(8,128)(2,1)} %bitcast.558, f32[1024,1408]{1,0:T(8,128)} %fusion.79, bf16[2048,2816]{1,0:T(8,128)(2,1)} %all-gather.12.cloned.1.call-done, f32[1024,2048]{1,0:T(8,128)} %get-tuple-element.310, f32[2048]{0:T(1024)S(1)} %convert_element_type.719, f32[1024]{0:T(1024)S(1)} %add_rsqrt_fusion.2), kind=kOutput, calls=%fused_computation.106 | convolution fusion | flops 11828199424 | bytes 29896704 | tf_op jit(solution)/shard_map/dot_general | solution.py:288
  423.7 46.8 %reduce-scatter.2.cloned.1.call-done = bf16[256,2048]{1,0:T(8,128)(2,1)} async-done(((bf16[1024,2048]{1,0:T(8,128)(2,1)}), bf16[256,2048]{1,0:T(8,128)(2,1)}) %reduce-scatter.2.cloned.1.call-update) | async-done | bytes 1048592 | tf_op jit(solution)/shard_map/reduce_scatter | solution.py:287
  470.6 1.5 fusion.90
  472.1 3.3 fusion.93
  (421 shorter events, 112.6 us)
Async XLA Ops:
  7.4 265.7 %copy-start = (bf16[256,2048]{1,0:T(8,128)(2,1)S(1)}, bf16[256,2048]{1,0:T(8,128)(2,1)}, u32[]{:S(2)}) copy-start(bf16[256,2048]{1,0:T(8,128)(2,1)} %param.46) | copy-start | bytes 3145732
  7.4 31.6 %copy-start.12 = (bf16[256]{0:T(256)(128)(2,1)S(1)}, bf16[256]{0:T(256)(128)(2,1)}, u32[]{:S(2)}) copy-start(bf16[256]{0:T(256)(128)(2,1)} %param.45) | copy-start | bytes 1540
  7.4 270.4 %all-gather.14.cloned.1.call-start = ((), (), s32[]{:S(2)}) async-start(), calls=%async_computation.4 | async-start | bytes 3063808 | tf_op jit(solution)/shard_map/all_gather | solution.py:84
  8.1 366.2 %all-reduce.8.cloned.1.call-start = ((), (), s32[]{:S(2)}) async-start(), calls=%async_computation.1 | async-start | bytes 8388608 | tf_op jit(solution)/shard_map/psum | solution.py:278
  9.0 32.0 %collective-permute-start = (bf16[3,256]{0,1:T(8,128)(2,1)S(1)}, bf16[3,256]{0,1:T(8,128)(2,1)S(1)}, u32[]{:S(2)}, u32[]{:S(2)}) collective-permute-start(bf16[3,256]{0,1:T(8,128)(2,1)S(1)} %copy.225), channel_id=1, source_target_pairs={{0,4},{4,8},{8,12},{12,16},{16,20},{20,24},{24,28},{28,32},{32,36}... | collective-permute-start | bytes 4616 | tf_op jit(solution)/shard_map/ppermute | solution.py:16
  14.7 25.6 %collective-permute-start.1 = (bf16[3,2,128]{2,0,1:T(4,128)(2,1)S(1)}, bf16[3,2,128]{2,0,1:T(4,128)(2,1)S(1)}, u32[]{:S(2)}, u32[]{:S(2)}) collective-permute-start(bf16[3,2,128]{2,0,1:T(4,128)(2,1)S(1)} %slice.452), channel_id=1, source_target_pairs={{0,4},{4,8},{8,12},{12,16},{16,20},{20,24},{24,28},{28,32},{32,36}... | collective-permute-start | bytes 4616 | tf_op jit(solution)/shard_map/ppermute | solution.py:16
  17.7 0.8 copy-start.5
  18.5 27.4 %collective-permute-start.2 = (bf16[3,2,128]{2,0,1:T(4,128)(2,1)S(1)}, bf16[3,2,128]{2,0,1:T(4,128)(2,1)S(1)}, u32[]{:S(2)}, u32[]{:S(2)}) collective-permute-start(bf16[3,2,128]{2,0,1:T(4,128)(2,1)S(1)} %slice.458), channel_id=1, source_target_pairs={{0,4},{4,8},{8,12},{12,16},{16,20},{20,24},{24,28},{28,32},{32,36}... | collective-permute-start | bytes 4616 | tf_op jit(solution)/shard_map/ppermute | solution.py:16
  23.0 111.7 %collective-permute-start.3 = (bf16[3,256]{0,1:T(8,128)(2,1)S(1)}, bf16[3,256]{0,1:T(8,128)(2,1)S(1)}, u32[]{:S(2)}, u32[]{:S(2)}) collective-permute-start(bf16[3,256]{0,1:T(8,128)(2,1)S(1)} %copy.239), channel_id=1, source_target_pairs={{0,4},{4,8},{8,12},{12,16},{16,20},{20,24},{24,28},{28,32},{32,36}... | collective-permute-start | bytes 4616 | tf_op jit(solution)/shard_map/ppermute | solution.py:16
  252.5 0.8 copy-start.4
  266.2 5.7 %copy-start.3 = (f32[1024,1,2,128]{0,3,2,1:T(8,128)S(1)}, f32[1024,1,2,128]{0,3,2,1:T(8,128)}, u32[]{:S(2)}) copy-start(f32[1024,1,2,128]{0,3,2,1:T(8,128)} %reshape.977) | copy-start | bytes 3145732
  272.7 1.7 copy-start.6
  277.6 0.9 copy-start.7
  277.6 1.0 copy-start.8
  277.6 2.1 copy-start.9
  277.6 2.1 copy-start.10
  277.7 106.1 %all-gather.16.cloned.1.call-start = ((), (), s32[]{:S(2)}) async-start(), calls=%async_computation.5 | async-start | bytes 8650752 | tf_op jit(solution)/shard_map/all_gather | solution.py:84
  278.4 111.1 %all-gather.12.cloned.1.call-start = ((), (), s32[]{:S(2)}) async-start(), calls=%async_computation.2 | async-start | bytes 11894784 | tf_op jit(solution)/shard_map/all_gather | solution.py:68
  279.4 191.1 %reduce-scatter.2.cloned.1.call-start = ((), (), s32[]{:S(2)}) async-start(), calls=%async_computation.3 | async-start | bytes 5242880 | tf_op jit(solution)/shard_map/reduce_scatter | solution.py:287
  374.3 3.4 copy-start.2
  402.2 21.6 %copy-start.11 = (bf16[2048]{0:T(1024)(128)(2,1)S(1)}, bf16[2048]{0:T(1024)(128)(2,1)}, u32[]{:S(2)}) copy-start(bf16[2048]{0:T(1024)(128)(2,1)} %param.53) | copy-start | bytes 12292
  402.2 73.2 %copy-start.1 = (bf16[256,2048]{1,0:T(8,128)(2,1)S(1)}, bf16[256,2048]{1,0:T(8,128)(2,1)}, u32[]{:S(2)}) copy-start(bf16[256,2048]{1,0:T(8,128)(2,1)} %param.46) | copy-start | bytes 3145732
Sparse Core Ops, SparseCore 0:
  10.3 49.5 all-gather.13
  280.1 23.3 all-gather.15
  305.8 61.5 all-gather.11
Sparse Core Ops, SparseCore 1:
  277.7 96.5 all-reduce.7
  423.8 46.7 reduce-scatter.1
where the time goes:
time: 490 us; the launch traced here: 482 us
  waiting for transfers between devices  143 us (29%)
  local copies, waits for them, and re-layouts  137 us (28%)
  matrix products  104 us (21%)
  other arithmetic  45 us (9%)
  blocking collectives  24.6 us (5%)
  between operations  15.1 us (3%)
  starting transfers between devices  12.4 us (3%)
    psum x1, waiting for transfers between devices, local(): mix = lax.psum(partial_value.astype(jnp.bfloat16), 'tp').astype(jnp.float32)  94.6 us
    dynamic_update_slice x32, local copies, waits for them, and re-layouts, block_pass(): end_state, (outputs, cumulative) = lax.scan(one_block, start_state, blocked)  83.5 us
    reduce_scatter x1, waiting for transfers between devices, local(): lax.psum_scatter(lax.dot_general(hidden, down_full, (((1,), (1,)), ((), (...  46.8 us
    all_gather x3, blocking collectives, collected_together(): both, at, found = (lax.all_gather(jnp.concatenate(lines), axis), 0, {})  24.6 us
    dot_general x1, matrix products, local(): lax.dot_general(hidden, down_full, (((1,), (1,)), ((), ())), preferred_el...  21.5 us
    dot_general x16, matrix products, one_block(): jnp.einsum('ghls,sghp->lghp', weights, block_values, preferred_element_ty...  17.7 us
    dot_general x16, matrix products, one_block(): jnp.einsum('lghp,lgn->ghpn', scaled.astype(jnp.bfloat16), block_keys, pre...  16.3 us
    dynamic_slice x48, local copies, waits for them, and re-layouts, block_pass(): end_state, (outputs, cumulative) = lax.scan(one_block, start_state, blocked)  15.4 us
  transfers between devices with their start and end apart: 9, of which 2 were waited for; matrix products, arithmetic and copies ran while one was open for 51% of the time, Pallas kernels for 0%

commit v1 on v0

--- a/solution.py
+++ b/solution.py
@@ -275,7 +275,9 @@
     partial_value = partial_value + jnp.dot(
         large_normed, large_out, preferred_element_type=jnp.float32
     )
-    mix = lax.psum(partial_value.astype(jnp.bfloat16), "tp").astype(jnp.float32)
+    mix = jnp.sum(lax.all_gather(partial_value.astype(jnp.bfloat16), "tp"), axis=0).astype(
+        jnp.float32
+    )
     mixed = residual.astype(jnp.float32) + unit_rms(mix) * mixer_gain.astype(jnp.float32)
     normed_in = (unit_rms(mixed) * ffn_in_gain.astype(jnp.float32)).astype(jnp.bfloat16)
     pieces = in_one_piece((gate_proj, up_proj), SP, 0, 1)

time: 490 us -> 619 us (1.26)
  waiting for transfers between devices: 143 us -> 239 us
  local copies, waits for them, and re-layouts: 137 us -> 159 us
  other arithmetic: 45 us -> 63.6 us
    all_gather x0 -> x1, waiting for transfers between devices: none -> 151 us  [local(): lax.all_gather(partial_value.astype(jnp.bfloat16), 'tp')]
    psum x1 -> x0, waiting for transfers between devices: 94.6 us -> none  [local(): mix = lax.psum(partial_value.astype(jnp.bfloat16), 'tp').astype(jnp.float32)]
    all_gather x1, waiting for transfers between devices: 0.01 us -> 42.1 us  [in_one_piece(): lax.all_gather(both, axis, axis=dim, tiled=True)]
    reduce_sum x0 -> x1, other arithmetic: none -> 12.1 us  [local(): jnp.sum(lax.all_gather(partial_value.astype(jnp.bfloat16), 'tp'), axis=0)]
    unnamed x42 -> x70, local copies, waits for them, and re-layouts: 12.9 us -> 12.8 us
  transfers between devices with their start and end apart: 9 -> 9, of which waited for: 2 -> 3; matrix products, arithmetic and copies ran while one was open for 51% -> 45% of each run, Pallas kernels for 0% -> 0%
where the time goes in v1:
time: 619 us; the launch traced here: 612 us
  waiting for transfers between devices  239 us (39%)
  local copies, waits for them, and re-layouts  159 us (26%)
  matrix products  98.3 us (16%)
  other arithmetic  63.6 us (10%)
  blocking collectives  24.4 us (4%)
  between operations  13.7 us (2%)
  starting transfers between devices  12.6 us (2%)
    all_gather x1, waiting for transfers between devices, local(): lax.all_gather(partial_value.astype(jnp.bfloat16), 'tp')  151 us
    dynamic_update_slice x32, local copies, waits for them, and re-layouts, block_pass(): end_state, (outputs, cumulative) = lax.scan(one_block, start_state, blocked)  83.9 us
    reduce_scatter x1, waiting for transfers between devices, local(): lax.psum_scatter(lax.dot_general(hidden, down_full, (((1,), (1,)), ((), (...  45.9 us
    all_gather x1, waiting for transfers between devices, in_one_piece(): lax.all_gather(both, axis, axis=dim, tiled=True)  42.1 us
    all_gather x3, blocking collectives, collected_together(): both, at, found = (lax.all_gather(jnp.concatenate(lines), axis), 0, {})  24.4 us
    dot_general x1, matrix products, local(): lax.dot_general(hidden, down_full, (((1,), (1,)), ((), ())), preferred_el...  21.6 us
    dynamic_slice x48, local copies, waits for them, and re-layouts, block_pass(): end_state, (outputs, cumulative) = lax.scan(one_block, start_state, blocked)  20.6 us
    dot_general x16, matrix products, one_block(): jnp.einsum('ghls,sghp->lghp', weights, block_values, preferred_element_ty...  17.7 us
  transfers between devices with their start and end apart: 9, of which 3 were waited for; matrix products, arithmetic and copies ran while one was open for 45% of the time, Pallas kernels for 0%

profile of v1, /device:TPU:1, one launch (start us, length us, event | category | flops | bytes accessed | tf_op | source)
XLA Modules:
  0.0 611.6 jit_solution(17465058946183061323)
XLA Ops:
  6.6 1.2 copy.231
  8.6 4.6 collective-permute-start.2
  15.7 1.9 collective-permute-start.1
  19.1 3.6 collective-permute-start
  24.1 1.9 collective-permute-start.3
  26.1 2.0 copy.226
  28.2 2.1 copy.240
  30.9 1.3 bitcast_convert_fusion.7
  32.2 1.4 slice_convert_fusion.7
  34.3 1.4 slice_convert_fusion.3
  37.2 1.3 fusion.178
  41.3 1.2 copy.248
  43.2 2.4 multiply_convert_fusion.9
  46.3 2.5 multiply_convert_fusion.10
  49.7 3.1 fusion.118
  53.8 88.3 %while.30 = (s32[]{:T(128)}, f32[1,4,64,128]{3,2,1,0:T(8,128)S(1)}, f32[8,128,1,4,64]{1,0,4,3,2:T(8,128)}, f32[8,128,1,4]{3,1,2,0:T(8,128)}, f32[8,128,1,4]{3,1,...) while((s32[]{:T(128)}, f32[1,4,64,128]{3,2,1,0:T(8,128)S(1)}, ...), condition=%wide.region_2.3_spmd.clone, body=%wide.region_0.2_spmd.clone.sunk | while | flops 30065156 | bytes 1597160 | solution.py:149
  57.5 1.1 fusion.250
  58.7 4.4 dynamic_update_slice.27
  68.6 1.1 fusion.250
  69.7 4.4 dynamic_update_slice.27
  80.8 4.4 dynamic_update_slice.27
  90.6 1.1 fusion.250
  91.8 4.4 dynamic_update_slice.27
  101.7 1.1 fusion.250
  102.8 4.4 dynamic_update_slice.27
  113.8 4.4 dynamic_update_slice.27
  123.7 1.1 fusion.250
  124.9 4.4 dynamic_update_slice.27
  135.9 4.4 dynamic_update_slice.27
  142.8 3.3 fusion.119
  147.1 90.4 %while.31 = (s32[]{:T(128)}, f32[1,2,128,128]{3,2,1,0:T(8,128)S(1)}, f32[8,128,1,2,128]{1,0,4,3,2:T(8,128)}, f32[8,128,1,2]{3,1,2,0:T(8,128)}, f32[8,128,1,2]{3,...) while((s32[]{:T(128)}, ...), condition=%wide.region_5.6_spmd.clone, body=%wide.region_3.5_spmd.clone.sunk | while | flops 29868292 | bytes 1569980 | solution.py:149
  151.9 4.8 dynamic_update_slice.29
  163.2 4.8 dynamic_update_slice.29
  174.6 4.8 dynamic_update_slice.29
  185.8 4.8 dynamic_update_slice.29
  197.2 4.8 dynamic_update_slice.29
  208.4 4.8 dynamic_update_slice.29
  219.7 4.8 dynamic_update_slice.29
  231.0 4.8 dynamic_update_slice.29
  238.4 2.7 all-gather.6
  241.8 10.9 %all-gather.7 = bf16[4,514,128]{2,1,0:T(8,128)(2,1)S(1)} all-gather(bf16[1,514,128]{2,1,0:T(8,128)(2,1)S(1)} %maximum_bitcast_fusion.1), channel_id=3, replica_groups=mesh['sp_0'=4,'sp_1'=4,'sp_2'=2,'tp'=4] {'sp_1'}, dimensions={0}, use_global_device_ids=true | all-gather | bytes 657920 | tf_op jit(solution)/shard_map/all_gather | solution.py:33
  255.1 10.8 %all-gather.8 = bf16[4,514,128]{2,1,0:T(8,128)(2,1)S(1)} all-gather(bf16[1,514,128]{2,1,0:T(8,128)(2,1)S(1)} %maximum_bitcast_fusion.2), channel_id=4, replica_groups=mesh['sp_0'=4,'sp_1'=4,'sp_2'=2,'tp'=4] {'sp_0'}, dimensions={0}, use_global_device_ids=true | all-gather | bytes 657920 | tf_op jit(solution)/shard_map/all_gather | solution.py:33
  267.7 1.9 add_exponential_fusion
  269.6 1.2 copy.252
  270.9 2.4 reshape.977
  278.7 1.9 add_exponential_fusion.1
  280.6 1.2 copy.247
  281.8 2.4 reshape.954
  286.0 1.5 fusion.135
  287.5 1.7 fusion.97
  290.7 1.5 fusion.141
  293.3 1.3 fusion.191
  294.7 3.3 add_convert_fusion
  299.2 5.7 copy.254
  304.9 151.3 %all-gather.16.cloned.1.call-done = bf16[4096,2048]{1,0:T(8,128)(2,1)} async-done(((bf16[1024,2048]{1,0:T(8,128)(2,1)}), bf16[4096,2048]{1,0:T(8,128)(2,1)}) %all-gather.16.cloned.1.call-update) | async-done | bytes 16777232 | tf_op jit(solution)/shard_map/all_gather | solution.py:278
  456.2 12.1 %reduce_sum.79 = bf16[1024,2048]{1,0:T(8,128)(2,1)} reduce(bf16[4,1024,2048]{2,1,0:T(8,128)(2,1)} %bitcast.555, bf16[]{:T(256)} %constant.118.clone.1), dimensions={0}, to_apply=%region_12.13 | reduce | flops 6291456 | bytes 20971522 | tf_op jit(solution)/shard_map/reduce_sum | solution.py:278
  468.3 3.4 fusion.74
  472.1 6.0 multiply_reduce_fusion
  478.1 42.1 %all-gather.14.cloned.1.call-done = bf16[2048,2816]{1,0:T(8,128)(2,1)} async-done(((bf16[64,2816]{1,0:T(8,128)(2,1)}), bf16[2048,2816]{1,0:T(8,128)(2,1)}) %all-gather.14.cloned.1.call-update) | async-done | bytes 11534352 | tf_op jit(solution)/shard_map/all_gather | solution.py:68
  520.2 12.5 %fusion.79 = f32[1024,1408]{1,0:T(8,128)} fusion(bf16[2048,2816]{1,0:T(8,128)(2,1)} %all-gather.14.cloned.1.call-done, f32[1024,2048]{1,0:T(8,128)} %get-tuple-element.310, f32[2048]{0:T(1024)S(1)} %convert_element_type.721, f32[1024]{0:T(1024)S(1)} %add_rsqrt_fusion.2), kind=kOutput, calls=%fused_computation.102 | convolution fusion | flops 5911871488 | bytes 19935232 | tf_op jit(solution)/shard_map/dot_general | solution.py:284
  532.8 21.6 %fusion.86 = bf16[1024,2048]{1,0:T(8,128)(2,1)} fusion(bf16[2048,1408]{1,0:T(8,128)(2,1)} %bitcast.560, f32[1024,1408]{1,0:T(8,128)} %fusion.79, bf16[2048,2816]{1,0:T(8,128)(2,1)} %all-gather.14.cloned.1.call-done, f32[1024,2048]{1,0:T(8,128)} %get-tuple-element.310, f32[2048]{0:T(1024)S(1)} %convert_element_type.721, f32[1024]{0:T(1024)S(1)} %add_rsqrt_fusion.2), kind=kOutput, calls=%fused_computation.106 | convolution fusion | flops 11828199424 | bytes 29896704 | tf_op jit(solution)/shard_map/dot_general | solution.py:290
  554.4 45.9 %reduce-scatter.2.cloned.1.call-done = bf16[256,2048]{1,0:T(8,128)(2,1)} async-done(((bf16[1024,2048]{1,0:T(8,128)(2,1)}), bf16[256,2048]{1,0:T(8,128)(2,1)}) %reduce-scatter.2.cloned.1.call-update) | async-done | bytes 1048592 | tf_op jit(solution)/shard_map/reduce_scatter | solution.py:289
  600.3 1.5 fusion.90
  601.8 3.3 fusion.93
  (450 shorter events, 132.6 us)
Async XLA Ops:
  6.5 286.8 %copy-start = (bf16[256,2048]{1,0:T(8,128)(2,1)S(1)}, bf16[256,2048]{1,0:T(8,128)(2,1)}, u32[]{:S(2)}) copy-start(bf16[256,2048]{1,0:T(8,128)(2,1)} %param.46) | copy-start | bytes 3145732
  6.5 34.0 %copy-start.8 = (bf16[1024,256]{1,0:T(8,128)(2,1)S(1)}, bf16[1024,256]{1,0:T(8,128)(2,1)}, u32[]{:S(2)}) copy-start(bf16[1024,256]{1,0:T(8,128)(2,1)} %param.35) | copy-start | bytes 1572868
  6.5 34.3 %copy-start.25 = (bf16[256]{0:T(256)(128)(2,1)S(1)}, bf16[256]{0:T(256)(128)(2,1)}, u32[]{:S(2)}) copy-start(bf16[256]{0:T(256)(128)(2,1)} %param.45) | copy-start | bytes 1540
  6.5 36.1 %copy-start.26 = (bf16[256]{0:T(256)(128)(2,1)S(1)}, bf16[256]{0:T(256)(128)(2,1)}, u32[]{:S(2)}) copy-start(bf16[256]{0:T(256)(128)(2,1)} %param.44) | copy-start | bytes 1540
  6.5 266.7 %all-gather.18.cloned.1.call-start = ((), (), s32[]{:S(2)}) async-start(), calls=%async_computation.4 | async-start | bytes 3063808 | tf_op jit(solution)/shard_map/all_gather | solution.py:84
  7.8 0.8 copy-start.6
  8.6 34.5 %collective-permute-start.2 = (bf16[3,2,128]{2,0,1:T(4,128)(2,1)S(1)}, bf16[3,2,128]{2,0,1:T(4,128)(2,1)S(1)}, u32[]{:S(2)}, u32[]{:S(2)}) collective-permute-start(bf16[3,2,128]{2,0,1:T(4,128)(2,1)S(1)} %slice.458), channel_id=1, source_target_pairs={{0,4},{4,8},{8,12},{12,16},{16,20},{20,24},{24,28},{28,32},{32,36}... | collective-permute-start | bytes 4616 | tf_op jit(solution)/shard_map/ppermute | solution.py:16
  14.3 0.8 copy-start.5
  15.7 30.6 %collective-permute-start.1 = (bf16[3,2,128]{2,0,1:T(4,128)(2,1)}, bf16[3,2,128]{2,0,1:T(4,128)(2,1)}, u32[]{:S(2)}, u32[]{:S(2)}) collective-permute-start(bf16[3,2,128]{2,0,1:T(4,128)(2,1)} %slice.452), channel_id=1, source_target_pairs={{0,4},{4,8},{8,12},{12,16},{16,20},{20,24},{24,28},{28,32},{32,36}... | collective-permute-start | bytes 4616 | tf_op jit(solution)/shard_map/ppermute | solution.py:16
  19.1 30.6 %collective-permute-start = (bf16[3,256]{0,1:T(8,128)(2,1)}, bf16[3,256]{0,1:T(8,128)(2,1)}, u32[]{:S(2)}, u32[]{:S(2)}) collective-permute-start(bf16[3,256]{0,1:T(8,128)(2,1)} %copy.225), channel_id=1, source_target_pairs={{0,4},{4,8},{8,12},{12,16},{16,20},{20,24},{24,28},{28,32},{32,36}... | collective-permute-start | bytes 4616 | tf_op jit(solution)/shard_map/ppermute | solution.py:16
  24.1 118.7 %collective-permute-start.3 = (bf16[3,256]{0,1:T(8,128)(2,1)}, bf16[3,256]{0,1:T(8,128)(2,1)}, u32[]{:S(2)}, u32[]{:S(2)}) collective-permute-start(bf16[3,256]{0,1:T(8,128)(2,1)} %copy.239), channel_id=1, source_target_pairs={{0,4},{4,8},{8,12},{12,16},{16,20},{20,24},{24,28},{28,32},{32,36}... | collective-permute-start | bytes 4616 | tf_op jit(solution)/shard_map/ppermute | solution.py:16
  26.1 273.2 %all-gather.20.cloned.1.call-start = ((), (), s32[]{:S(2)}) async-start(), calls=%async_computation.5 | async-start | bytes 8650752 | tf_op jit(solution)/shard_map/all_gather | solution.py:84
  254.6 26.0 %copy-start.11 = (f32[256]{0:T(256)}, f32[256]{0:T(256)S(1)}, u32[]{:S(2)}) copy-start(f32[256]{0:T(256)S(1)} %broadcast_bitcast_fusion.7) | copy-start | bytes 3076
  254.7 25.9 %copy-start.12 = (f32[256]{0:T(256)}, f32[256]{0:T(256)S(1)}, u32[]{:S(2)}) copy-start(f32[256]{0:T(256)S(1)} %broadcast_bitcast_fusion.8) | copy-start | bytes 3076
  254.8 25.8 %copy-start.13 = (f32[256]{0:T(256)}, f32[256]{0:T(256)S(1)}, u32[]{:S(2)}) copy-start(f32[256]{0:T(256)S(1)} %broadcast_bitcast_fusion.9) | copy-start | bytes 3076
  255.1 21.2 %copy-start.24 = (f32[1,4]{1,0:T(1,128)S(1)}, f32[1,4]{1,0:T(1,128)}, u32[]{:S(2)}) copy-start(f32[1,4]{1,0:T(1,128)} %get-tuple-element.315) | copy-start | bytes 52
  265.9 0.8 copy-start.4
  273.3 183.0 %all-gather.16.cloned.1.call-start = ((), (), s32[]{:S(2)}) async-start(), calls=%async_computation.3 | async-start | bytes 20971520 | tf_op jit(solution)/shard_map/all_gather | solution.py:278
  284.2 6.4 %copy-start.14 = (f32[256]{0:T(256)S(1)}, f32[256]{0:T(256)}, u32[]{:S(2)}) copy-start(f32[256]{0:T(256)} %mul.1072) | copy-start | bytes 3076
  284.2 6.5 %copy-start.15 = (f32[256]{0:T(256)S(1)}, f32[256]{0:T(256)}, u32[]{:S(2)}) copy-start(f32[256]{0:T(256)} %mul.1076) | copy-start | bytes 3076
  284.2 6.5 %copy-start.16 = (f32[256]{0:T(256)S(1)}, f32[256]{0:T(256)}, u32[]{:S(2)}) copy-start(f32[256]{0:T(256)} %mul.1081) | copy-start | bytes 3076
  284.2 6.5 %copy-start.17 = (f32[256]{0:T(256)S(1)}, f32[256]{0:T(256)}, u32[]{:S(2)}) copy-start(f32[256]{0:T(256)} %mul.1086) | copy-start | bytes 3076
  284.2 6.5 %copy-start.18 = (f32[256]{0:T(256)S(1)}, f32[256]{0:T(256)}, u32[]{:S(2)}) copy-start(f32[256]{0:T(256)} %mul.1103) | copy-start | bytes 3076
  284.2 6.5 %copy-start.19 = (f32[256]{0:T(256)S(1)}, f32[256]{0:T(256)}, u32[]{:S(2)}) copy-start(f32[256]{0:T(256)} %mul.1091) | copy-start | bytes 3076
  284.2 8.0 %copy-start.3 = (f32[1024,1,4,64]{0,3,2,1:T(8,128)S(1)}, f32[1024,1,4,64]{0,3,2,1:T(8,128)}, u32[]{:S(2)}) copy-start(f32[1024,1,4,64]{0,3,2,1:T(8,128)} %reshape.954) | copy-start | bytes 3145732
  286.0 6.9 %copy-start.23 = (f32[256]{0:T(256)S(1)}, f32[256]{0:T(256)}, u32[]{:S(2)}) copy-start(f32[256]{0:T(256)} %convert_element_type.699) | copy-start | bytes 3076
  293.0 1.7 copy-start.7
  294.7 3.4 copy-start.9
  294.7 3.4 copy-start.10
  294.7 4.5 copy-start.20
  294.7 4.5 copy-start.21
  298.0 222.2 %all-gather.14.cloned.1.call-start = ((), (), s32[]{:S(2)}) async-start(), calls=%async_computation.1 | async-start | bytes 11894784 | tf_op jit(solution)/shard_map/all_gather | solution.py:68
  298.9 301.4 %reduce-scatter.2.cloned.1.call-start = ((), (), s32[]{:S(2)}) async-start(), calls=%async_computation.2 | async-start | bytes 5242880 | tf_op jit(solution)/shard_map/reduce_scatter | solution.py:289
  468.3 3.8 copy-start.2
  532.8 21.7 %copy-start.22 = (bf16[2048]{0:T(1024)(128)(2,1)S(1)}, bf16[2048]{0:T(1024)(128)(2,1)}, u32[]{:S(2)}) copy-start(bf16[2048]{0:T(1024)(128)(2,1)} %param.53) | copy-start | bytes 12292
  532.8 72.3 %copy-start.1 = (bf16[256,2048]{1,0:T(8,128)(2,1)S(1)}, bf16[256,2048]{1,0:T(8,128)(2,1)}, u32[]{:S(2)}) copy-start(bf16[256,2048]{1,0:T(8,128)(2,1)} %param.46) | copy-start | bytes 3145732
Sparse Core Ops, SparseCore 0:
  26.2 47.8 all-gather.17
  273.4 23.3 all-gather.19
  298.5 157.7 all-gather.15
  458.4 61.8 all-gather.13
  554.5 45.7 reduce-scatter.1
